TPU v7x, 32 devices: a whole 2x2x4 slice. The times are simulated.
32 devices in a mesh: ra: 8 (over z, y), cb: 4 (over x, core).
Axes of the slice: x: 2, y: 2, z: 4, core: 2. Of those that a mesh axis runs over, the one named last changes fastest.
Arguments:
- tokens: bfloat16 [512, 4096], P(None, 'ra'), may hold values from -4 to 4, as said below
- pre_gain_first: float32 [4096], P('ra'), may hold values from 0.1 to 1.9
- gate_first: bfloat16 [4096, 11264], P('ra', 'cb'), may hold values from -0.125 to 0.125
- up_first: bfloat16 [4096, 11264], P('ra', 'cb'), may hold values from -0.125 to 0.125
- down_first: bfloat16 [11264, 4096], P('cb', 'ra'), may hold values from -0.078125 to 0.078125
- post_gain_first: float32 [4096], P('ra'), may hold values from 0.1 to 1.9
- pre_gain_second: float32 [4096], P('ra'), may hold values from 0.1 to 1.9
- gate_second: bfloat16 [4096, 11264], P('ra', 'cb'), may hold values from -0.125 to 0.125
- up_second: bfloat16 [4096, 11264], P('ra', 'cb'), may hold values from -0.125 to 0.125
- down_second: bfloat16 [11264, 4096], P('cb', 'ra'), may hold values from -0.078125 to 0.078125
- post_gain_second: float32 [4096], P('ra'), may hold values from 0.1 to 1.9
Outputs:
- mixed: bfloat16 [512, 4096], P(None, 'ra')
Inputs may be any that keep to these rules, and one draw needn't show every extreme that they name: `tokens`: each block of 128 consecutive channels has its own scale, and rows have their own scales.
All inputs are finite; a program needn't handle non-finite values.
Results may differ from a plain program's by a relative error of at most 0.0071.
Values may be sent and summed in bfloat16 or wider, within the bound.
A program may use at most 64 MiB of HBM per device.

v0:
```python
import functools

import jax
import jax.numpy as jnp
from jax import lax
from jax.experimental import pallas as pl
from jax.experimental.pallas import tpu as pltpu
from jax.sharding import PartitionSpec as P

EPS = 1e-06
MESH = pl.DeviceIdType.MESH
F32 = jnp.float32
BF16 = jnp.bfloat16


def log2(n):
    return n.bit_length() - 1


def bits_of(index, count):
    return [lax.rem(index // (1 << b), 2) for b in range(count)]


def spread(col, lanes):
    return jnp.broadcast_to(col, (col.shape[0], 128)).T[0:8]


def column(row):
    return jnp.broadcast_to(row[0:1], (128, row.shape[1])).T


def half_step(
    first, n, nc, width, *refs
):
    k, kc = log2(n), log2(nc)
    (h_ref, resid_ref, ss_ref, post_ref, pre_ref, gate_hbm, up_hbm, down_hbm), refs = refs[:8], refs[8:]
    if first:
        (h_out, mid_out, ss_out), refs = refs[:3], refs[3:]
    else:
        (y_out,), refs = refs[:1], refs[1:]
    (both_v, down_v, acc, hid, branch, scale, ss_slots, br_slots, br_send, ag, ss_all), refs = refs[:11], refs[11:]
    snd, refs = refs[:k], refs[k:]
    rcv, refs = refs[:k], refs[k:]
    csnd, refs = refs[:kc], refs[kc:]
    crcv, refs = refs[:kc], refs[kc:]
    (w_sem, rs_s, rs_r, ag_s, ag_r, c_s, c_r, ss_s, ss_r, br_s, br_r, cg_s, cg_r, cs_s, cs_r) = refs

    tokens, depth = h_ref.shape
    chunks, cw, _ = down_v.shape
    me, col = lax.axis_index("ra"), lax.axis_index("cb")
    eb, xb = bits_of(me, k), bits_of(col, kc)
    partners = [me + (1 - 2 * eb[b]) * (1 << b) for b in range(k)]
    cpartners = [col + (1 - 2 * xb[b]) * (1 << b) for b in range(kc)]
    crows = tokens // nc

    def weights(c):
        cols = pl.ds(pl.multiple_of(c * cw, 128), cw)
        return [
            pltpu.make_async_copy(gate_hbm.at[:, cols], both_v.at[c, :, pl.ds(0, cw)], w_sem.at[0, c]),
            pltpu.make_async_copy(up_hbm.at[:, cols], both_v.at[c, :, pl.ds(cw, cw)], w_sem.at[1, c]),
            pltpu.make_async_copy(down_hbm.at[cols, :], down_v.at[c], w_sem.at[2, c]),
        ]

    @pl.loop(0, chunks)
    def _(c):
        for copy in weights(c):
            copy.start()

    barrier = pltpu.get_barrier_semaphore()

    def xor(index, bits, off):
        out = index
        for b, bit in enumerate(bits):
            if (off >> b) & 1:
                out = out + (1 - 2 * bit) * (1 << b)
        return out

    for off in range(1, n):
        pl.semaphore_signal(barrier, inc=1, device_id={"ra": xor(me, eb, off)}, device_id_type=MESH)
    for off in range(1, nc):
        pl.semaphore_signal(barrier, inc=1, device_id={"cb": xor(col, xb, off)}, device_id_type=MESH)
    pl.semaphore_wait(barrier, n - 1 + nc - 1)

    def remote(src, dst, s, r, **where):
        return pltpu.make_async_remote_copy(
            src_ref=src, dst_ref=dst, send_sem=s, recv_sem=r, device_id=where, device_id_type=MESH
        )

    def ss_copy(off):
        return remote(ss_ref, ss_slots.at[off - 1], ss_s.at[off - 1], ss_r.at[off - 1], ra=xor(me, eb, off))

    for off in range(1, n):
        ss_copy(off).start()

    def plan(c):
        swap = jnp.where(lax.rem(c, 3) == 1, 1, 0)
        bits, to = list(eb), list(partners)
        if k > 1:
            bits[0], bits[1] = eb[0] + swap * (eb[1] - eb[0]), eb[1] + swap * (eb[0] - eb[1])
            to[0] = partners[0] + swap * (partners[1] - partners[0])
            to[1] = partners[1] + swap * (partners[0] - partners[1])
        return bits, to

    def rows_at(base, size):
        return pl.ds(pl.multiple_of(base, size), size)

    def rs_copy(c, s, to):
        return remote(snd[s].at[c], rcv[s].at[c], rs_s.at[s, c], rs_r.at[s, c], ra=to[s])

    def ag_copy(c, s, bits, to):
        size = tokens >> (s + 1)
        base = sum(bits[i] * (tokens >> (i + 1)) for i in range(s + 1))
        part = hid.at[c, rows_at(base, size), :]
        return remote(part, part, ag_s.at[s, c], ag_r.at[s, c], ra=to[s])

    branch[...] = jnp.zeros_like(branch)

    lags = [2 * i for i in range(2 * k + 1)]

    def tick(t, carry):
        @pl.when(t < chunks)
        def _():
            c = t
            bits, to = plan(c)
            gate_copy, up_copy, _ = weights(c)
            gate_copy.wait()
            up_copy.wait()
            half = tokens // 2
            theirs = h_ref[rows_at((1 - bits[0]) * half, half), :]
            snd[0][c] = jnp.dot(theirs, both_v[c], preferred_element_type=F32).astype(BF16)
            rs_copy(c, 0, to).start()
            mine = h_ref[rows_at(bits[0] * half, half), :]
            acc[c] = jnp.dot(mine, both_v[c], preferred_element_type=F32)

        for s in range(1, k):
            rs_lag = lags[s]
            @pl.when((t >= rs_lag) & (t < chunks + rs_lag))
            def _():
                c = t - rs_lag
                bits, to = plan(c)
                rs_copy(c, s - 1, to).wait()
                size = tokens >> (s + 1)
                base = sum(bits[i] * (tokens >> (i + 1)) for i in range(1, s))
                out = (1 - bits[s]) * size
                snd[s][c] = (
                    acc[c, rows_at(base + out, size), :] + rcv[s - 1][c, rows_at(out, size), :].astype(F32)
                ).astype(BF16)
                rs_copy(c, s, to).start()
                keep = bits[s] * size
                acc[c, rows_at(base + keep, size), :] += rcv[s - 1][c, rows_at(keep, size), :].astype(F32)

        @pl.when(t == lags[k])
        def _():
            for off in range(1, n):
                ss_copy(off).wait()
            total = ss_ref[...]
            for off in range(1, n):
                total = total + ss_slots[off - 1]
            for b in range(nc):
                scale[b * crows : (b + 1) * crows, :] = column(lax.rsqrt(total[b] / width + EPS))

        @pl.when((t >= lags[k]) & (t < chunks + lags[k]))
        def _():
            c = t - lags[k]
            bits, to = plan(c)
            rs_copy(c, k - 1, to).wait()
            size = tokens >> k
            base = sum(bits[i] * (tokens >> (i + 1)) for i in range(1, k))
            value = acc[c, rows_at(base, size), :] + rcv[k - 1][c].astype(F32)
            rows = rows_at(base + bits[0] * (tokens // 2), size)
            factor = scale[rows, 0:1]
            g, u = value[:, :cw] * factor, value[:, cw:] * factor
            hid[c, rows, :] = (g / (1.0 + jnp.exp(-g)) * u).astype(BF16)
            ag_copy(c, k - 1, bits, to).start()

        for s in range(k - 1, 0, -1):
            lag = lags[2 * k - s]
            @pl.when((t >= lag) & (t < chunks + lag))
            def _():
                c = t - lag
                bits, to = plan(c)
                ag_copy(c, s, bits, to).wait()
                ag_copy(c, s - 1, bits, to).start()

        @pl.when(t >= lags[2 * k])
        def _():
            c = t - lags[2 * k]
            bits, to = plan(c)
            ag_copy(c, 0, bits, to).wait()
            weights(c)[2].wait()
            branch[...] += jnp.dot(hid[c], down_v[c], preferred_element_type=F32)

        return carry

    lax.fori_loop(0, chunks + lags[2 * k], tick, 0)

    def c_copy(s):
        return remote(csnd[s], crcv[s], c_s.at[s], c_r.at[s], cb=cpartners[s])

    base = 0
    for s in range(kc):
        size = tokens >> (s + 1)
        out, keep = (1 - xb[s]) * size, xb[s] * size
        mine = branch[rows_at(base + out, size), :]
        if s:
            mine = mine + crcv[s - 1][rows_at(out, size), :].astype(F32)
        csnd[s][...] = mine.astype(csnd[s].dtype)
        c_copy(s).start()
        if s:
            branch[rows_at(base + keep, size), :] += crcv[s - 1][rows_at(keep, size), :].astype(F32)
        c_copy(s).wait()
        base = base + keep
    own = rows_at(base, crows)
    total = branch[own, :] + crcv[kc - 1][...].astype(F32)

    br_send[...] = spread(jnp.sum(total * total, axis=1, keepdims=True), crows)

    def br_copy(off):
        return remote(br_send, br_slots.at[off - 1], br_s.at[off - 1], br_r.at[off - 1], ra=xor(me, eb, off))

    for off in range(1, n):
        br_copy(off).start()
    squares = br_send[...]
    for off in range(1, n):
        br_copy(off).wait()
        squares = squares + br_slots[off - 1]
    factor = column(0.5 * lax.rsqrt(squares / width + EPS))[:, 0:1]
    resid = resid_ref[own, :].astype(F32) if first else resid_ref[...]
    middle = resid + factor * total * post_ref[...]
    if first:
        ag[own, :] = (middle * pre_ref[...]).astype(BF16)
        mid_out[...] = middle
    else:
        ag[own, :] = middle.astype(BF16)

    bases = [0]
    for s in range(kc):
        bases.append(bases[-1] + xb[s] * (tokens >> (s + 1)))

    def cg_copy(s):
        part = ag.at[rows_at(bases[s + 1], tokens >> (s + 1)), :]
        return remote(part, part, cg_s.at[s], cg_r.at[s], cb=cpartners[s])

    cg_copy(kc - 1).start()
    if first:
        block = sum(xb[s] * (nc >> (s + 1)) for s in range(kc))
        ss_all[block] = spread(jnp.sum(middle * middle, axis=1, keepdims=True), crows)

        def cs_copy(off):
            part = ss_all.at[block]
            return remote(part, part, cs_s.at[off - 1], cs_r.at[off - 1], cb=xor(col, xb, off))

        for off in range(1, nc):
            cs_copy(off).start()
    for s in range(kc - 1, -1, -1):
        cg_copy(s).wait()
        if s:
            cg_copy(s - 1).start()
    if first:
        for off in range(1, nc):
            cs_copy(off).wait()
        ss_out[...] = ss_all[...]
        h_out[...] = ag[...]
    else:
        y_out[...] = ag[...]


def run(first, n, nc, width, h, resid, ss, post, pre, gate, up, down):
    tokens, depth = h.shape
    hidden = gate.shape[1]
    cw = 256 if hidden % 256 == 0 else 128
    chunks = hidden // cw
    k, kc, crows = log2(n), log2(nc), tokens // nc
    vmem = pl.BlockSpec(memory_space=pltpu.VMEM)
    hbm = pl.BlockSpec(memory_space=pl.ANY)
    dma = pltpu.SemaphoreType.DMA
    if first:
        out = [
            jax.ShapeDtypeStruct((tokens, depth), BF16),
            jax.ShapeDtypeStruct((crows, depth), F32),
            jax.ShapeDtypeStruct((nc, 8, crows), F32),
        ]
    else:
        out = [jax.ShapeDtypeStruct((tokens, depth), BF16)]
    scratch = [
        pltpu.VMEM((chunks, depth, 2 * cw), BF16),
        pltpu.VMEM((chunks, cw, depth), BF16),
        pltpu.VMEM((chunks, tokens // 2, 2 * cw), F32),
        pltpu.VMEM((chunks, tokens, cw), BF16),
        pltpu.VMEM((tokens, depth), F32),
        pltpu.VMEM((tokens, 128), F32),
        pltpu.VMEM((n - 1, nc, 8, crows), F32),
        pltpu.VMEM((n - 1, 8, crows), F32),
        pltpu.VMEM((8, crows), F32),
        pltpu.VMEM((tokens, depth), BF16),
        pltpu.VMEM((nc, 8, crows), F32),
    ]
    scratch += [pltpu.VMEM((chunks, tokens >> (s + 1), 2 * cw), BF16) for s in range(k)] * 2
    scratch += [pltpu.VMEM((tokens >> (s + 1), depth), BF16 if s else F32) for s in range(kc)] * 2
    scratch += [dma((3, chunks))] + [dma((k, chunks))] * 4 + [dma((kc,))] * 2
    scratch += [dma((n - 1,))] * 4 + [dma((kc,))] * 2 + [dma((nc - 1,))] * 2
    return pl.pallas_call(
        functools.partial(half_step, first, n, nc, width),
        out_shape=out,
        in_specs=[vmem] * 5 + [hbm] * 3,
        out_specs=[vmem] * len(out),
        scratch_shapes=scratch,
        compiler_params=pltpu.CompilerParams(
            collective_id=0 if first else 1, has_side_effects=True, vmem_limit_bytes=60 * 1024 * 1024
        ),
        name="first" if first else "second",
    )(h, resid, ss, post, pre, gate, up, down)


def solution(mesh):
    n, nc = mesh.shape["ra"], mesh.shape["cb"]

    def body(tokens, pre1, gate1, up1, down1, post1, pre2, gate2, up2, down2, post2):
        count, depth = tokens.shape
        width = depth * n
        resid = tokens.astype(F32)
        squares = jnp.sum(resid * resid, axis=1).reshape(nc, 1, count // nc)
        ss = jnp.broadcast_to(squares, (nc, 8, count // nc))
        h = (resid * pre1[None, :]).astype(BF16)
        row = lambda gain: gain.reshape(1, depth)
        h2, mid, ss2 = run(True, n, nc, width, h, tokens, ss, row(post1), row(pre2), gate1, up1, down1)
        (out,) = run(False, n, nc, width, h2, mid, ss2, row(post2), row(pre2), gate2, up2, down2)
        return out

    in_specs = (
        P(None, "ra"), P("ra"), P("ra", "cb"), P("ra", "cb"), P("cb", "ra"), P("ra"),
        P("ra"), P("ra", "cb"), P("ra", "cb"), P("cb", "ra"), P("ra"),
    )
    return jax.shard_map(body, mesh=mesh, in_specs=in_specs, out_specs=P(None, "ra"), check_vma=False)
```

profile of v0, /device:TPU:0, one launch (start us, length us, event | category | flops | bytes accessed | tf_op | source)
XLA Modules:
  0.0 240.4 jit_solution(5738517245608402508)
XLA Ops:
  0.0 2.0 fusion.1
  2.0 0.6 broadcast_in_dim.9.refs_2_
  2.6 119.2 %first.1 = (bf16[512,512]{1,0:T(8,128)(2,1)}, f32[128,512]{1,0:T(8,128)}, f32[4,8,128]{2,1,0:T(8,128)}) custom-call(bf16[512,512]{1,0:T(8,128)(2,1)} %get-tuple-element.12.refs_0_, bf16[512,512]{1,0:T(8,128)(2,1)} %refs_1_.1, f32[4,8,128]{2,1,0:T(8,128)} %broadcast_in_dim.9.refs_2_, f32[1,512]{1,0:T(1,128)} %bitcast.7, f32[1,512]{1,0:T(1,128)} %bitcast.4, ...), custom_call_target="tpu_custom_call" | custom-call | tf_op jit(solution)/shard_map/first/pallas_call | solution.py:302
  121.8 116.8 %second.1 = bf16[512,512]{1,0:T(8,128)(2,1)} custom-call(bf16[512,512]{1,0:T(8,128)(2,1)} %get-tuple-element.8.refs_0_, f32[128,512]{1,0:T(8,128)} %get-tuple-element.9.refs_1_, f32[4,8,128]{2,1,0:T(8,128)} %get-tuple-element.10.refs_2_, f32[1,512]{1,0:T(1,128)} %bitcast.8, f32[1,512]{1,0:T(1,128)} %bitcast.5, bf16[512,2816]{1,0:T(8,128)(2,1)} %refs_5_.3, ...), custom_call_target="tpu_custom_call" | custom-call | tf_op jit(solution)/shard_map/second/pallas_call | solution.py:302
  238.6 1.9 copy.13
where the time goes:
time: 241 us; the launch traced here: 240 us
  Pallas kernels  236 us (98%)
  local copies, waits for them, and re-layouts  2.47 us (1%)
    pallas_call x2, Pallas kernels, run(): pl.pallas_call(functools.partial(half_step, first, n, nc, width), out_sha...  236 us

commit v1 on v0

v1 whole, which is shorter than its diff:
```python
import functools

import jax
import jax.numpy as jnp
from jax import lax
from jax.experimental import pallas as pl
from jax.experimental.pallas import tpu as pltpu
from jax.sharding import PartitionSpec as P

EPS = 1e-06
MESH = pl.DeviceIdType.MESH
F32 = jnp.float32
BF16 = jnp.bfloat16
LY, LZ = 3, 3
POST = (2, 3, 2, 3)


def log2(n):
    return n.bit_length() - 1


def spread(col):
    return jnp.broadcast_to(col, (col.shape[0], 128)).T[0:8]


def column(row):
    return jnp.broadcast_to(row[0:1], (128, row.shape[1])).T


class Plan:
    def __init__(self, n, nc, tokens, depth, hidden):
        self.n, self.nc, self.tokens, self.depth = n, nc, tokens, depth
        self.ny = 1 << (log2(n) // 2)
        self.nz = n // self.ny
        self.kx = log2(nc) - 1
        self.tb = 64 * self.ny
        self.half, self.g = self.tb // 2, 16
        self.cw = 256 if hidden % 256 == 0 else 128
        self.chunks, self.blocks = hidden // self.cw, tokens // self.tb
        self.items = self.chunks * self.blocks
        self.act = (self.nz - 1) * LZ + LY
        self.down = self.act + LY + (self.nz - 1) * LZ
        steps = [0, POST[0]] + [POST[1]] * self.kx + [POST[2], POST[3]]
        self.post = [self.down + sum(steps[: i + 1]) for i in range(len(steps))]
        self.gap = max(0, self.chunks + self.post[-1] - self.items)
        self.ticks = 2 * self.items + self.gap + self.post[-1]


def kernel(p, width, *refs):
    (tok, pre1, post1, pre2, post2, gate1, up1, down1, gate2, up2, down2, y_out), refs = refs[:12], refs[12:]
    (both_v, down_v, h_v, mid, acc, branch, scale, hid), refs = refs[:8], refs[8:]
    (y1_snd, y1_rcv, ca_snd, ca_rcv, cb_snd, cb_rcv, y2_snd, y2_rcv), refs = refs[:8], refs[8:]
    (d_rcv, x_snd, x_rcv, tot, br_snd, br_rcv, ms_snd, ms_rcv), refs = refs[:8], refs[8:]
    (w_sem, y1_s, y1_r, ca_s, ca_r, cb_s, cb_r, y2_s, y2_r, h2_s, h2_r, ga_s, ga_r, gb_s, gb_r, h1_s, h1_r), refs = (
        refs[:17], refs[17:],
    )
    d_s, d_r, x_s, x_r, t_s, t_r, br_s, br_r, ms_s, ms_r = refs

    n, nc, ny, nz, tb, half, g, cw = p.n, p.nc, p.ny, p.nz, p.tb, p.half, p.g, p.cw
    chunks, blocks, items = p.chunks, p.blocks, p.items
    me, col = lax.axis_index("ra"), lax.axis_index("cb")
    z, y = lax.div(me, ny), lax.rem(me, ny)
    core = lax.rem(col, 2)
    brow = ny * g

    def remote(src, dst, s, r, **where):
        return pltpu.make_async_remote_copy(
            src_ref=src, dst_ref=dst, send_sem=s, recv_sem=r, device_id=where, device_id_type=MESH
        )

    def rows(base, size):
        return pl.ds(pl.multiple_of(base, 16), size)

    def weights(layer, c):
        cols = pl.ds(pl.multiple_of(c * cw, 128), cw)
        gate, up, down = ((gate1, up1, down1), (gate2, up2, down2))[layer]
        k = layer * chunks + c
        return [
            pltpu.make_async_copy(gate.at[:, cols], both_v.at[k, :, pl.ds(0, cw)], w_sem.at[0, k]),
            pltpu.make_async_copy(up.at[:, cols], both_v.at[k, :, pl.ds(cw, cw)], w_sem.at[1, k]),
            pltpu.make_async_copy(down.at[cols, :], down_v.at[k], w_sem.at[2, k]),
        ]

    for layer in range(2):
        @pl.loop(0, chunks)
        def _(c):
            for copy in weights(layer, c):
                copy.start()

    barrier = pltpu.get_barrier_semaphore()
    for off in range(1, n):
        pl.semaphore_signal(barrier, inc=1, device_id={"ra": lax.rem(me + off, n)}, device_id_type=MESH)
    for off in range(1, nc):
        pl.semaphore_signal(barrier, inc=1, device_id={"cb": lax.rem(col + off, nc)}, device_id_type=MESH)

    def other_y(j):
        return z * ny + lax.rem(y + j, ny)

    def next_z(e):
        return lax.rem(z + (1 if e else nz - 1), nz) * ny + y

    def back_z(e):
        return lax.rem(z + (nz - 1 if e else 1), nz) * ny + y

    def place(e):
        return z if e else nz - 1 - z

    def y1_copy(s, j):
        return remote(
            y1_snd.at[s, j - 1], y1_rcv.at[s, ny - 1 - j], y1_s.at[j - 1, s], y1_r.at[ny - 1 - j, s], ra=other_y(j)
        )

    def ca_copy(s, e):
        return remote(ca_snd.at[s, e], ca_rcv.at[s, e], ca_s.at[e, s], ca_r.at[e, s], ra=next_z(e))

    def cb_copy(s, e):
        return remote(cb_snd.at[s, e], cb_rcv.at[s, e], cb_s.at[e, s], cb_r.at[e, s], ra=next_z(e))

    def y2_copy(s, j):
        return remote(
            y2_snd.at[s, j - 1], y2_rcv.at[s, ny - 1 - j], y2_s.at[j - 1, s], y2_r.at[ny - 1 - j, s], ra=other_y(j)
        )

    def h2_copy(s, base, j, owner):
        part = hid.at[s, rows(base + owner * g, g), :]
        return remote(part, part, h2_s.at[j - 1, s], h2_r.at[ny - 1 - j, s], ra=other_y(j))

    def ga_copy(s, e):
        part = hid.at[s, pl.ds(e * half + brow, g), :]
        return remote(part, part, ga_s.at[e, s], ga_r.at[e, s], ra=back_z(e))

    def gb_copy(s, e):
        part = hid.at[s, pl.ds(e * half, brow), :]
        return remote(part, part, gb_s.at[e, s], gb_r.at[e, s], ra=back_z(e))

    def h1_copy(s, e, j):
        return remote(
            hid.at[s, pl.ds(e * half + brow, g), :],
            hid.at[s, pl.ds(e * half + brow + (ny - j) * g, g), :],
            h1_s.at[e, j - 1, s], h1_r.at[e, ny - 1 - j, s], ra=other_y(j),
        )

    def ms_copy(layer, b, off):
        return remote(
            ms_snd.at[layer, b], ms_rcv.at[layer, b, n - 1 - off],
            ms_s.at[layer, b, off - 1], ms_r.at[layer, b, n - 1 - off], ra=lax.rem(me + off, n),
        )

    def br_copy(layer, b, off):
        return remote(
            br_snd.at[layer, b], br_rcv.at[layer, b, n - 1 - off],
            br_s.at[layer, b, off - 1], br_r.at[layer, b, n - 1 - off], ra=lax.rem(me + off, n),
        )

    def store_h(b, value):
        value = value.astype(BF16)
        for e in range(2):
            h_v[rows(b * tb + e * half, brow), :] = value[e * half : e * half + brow]
            for yy in range(ny):
                slot = lax.rem(yy - y + ny, ny)
                at = e * half + brow + yy * g
                h_v[rows(b * tb + e * half + brow + slot * g, g), :] = value[at : at + g]

    def squares(value):
        return spread(jnp.sum(value * value, axis=1, keepdims=True))

    def block_rows(b):
        return pl.ds(pl.multiple_of(b * tb, tb), tb)

    def start_blocks(b):
        value = tok[block_rows(b), :].astype(F32)
        mid[block_rows(b), :] = value
        ms_snd[0, b] = squares(value)

    for b in range(blocks):
        start_blocks(b)
    store_h(0, mid[0:tb, :] * pre1[...])

    pl.semaphore_wait(barrier, n - 1 + nc - 1)
    for b in range(blocks):
        for off in range(1, n):
            ms_copy(0, b, off).start()

    def factor_of(snd, rcv, copy, layer, b):
        for off in range(1, n):
            copy(layer, b, off).wait()
        total = snd[layer, b]
        for off in range(1, n):
            total = total + rcv[layer, b, off - 1]
        return column(lax.rsqrt(total / width + EPS))

    def prepare():
        for b in range(blocks):
            factor = factor_of(ms_snd, ms_rcv, ms_copy, 0, b)
            if b == 0:
                scale[block_rows(b), :] = factor
            else:
                scale[block_rows(b), :] = jnp.ones_like(factor)
                store_h(b, mid[block_rows(b), :] * factor[:, 0:1] * pre1[...])

    is_end = (z == 0) | (z == nz - 1)
    end_base = jnp.where(z == 0, 0, half)

    def item(u):
        later = u >= items + p.gap
        valid = ((u >= 0) & (u < items)) | (later & (u < 2 * items + p.gap))
        s = u - jnp.where(later, items + p.gap, 0)
        layer = jnp.where(later, 1, 0)
        b = lax.div(s, chunks)
        return valid, s, layer, b, s - b * chunks

    def tick(t, carry):
        @pl.when(t == chunks // 2)
        def _():
            prepare()

        valid, s, layer, b, c = item(t)

        @pl.when(valid)
        def _():
            for one in range(2):
                @pl.when((b == 0) & (layer == one))
                def _():
                    gate_copy, up_copy, _ = weights(one, c)
                    gate_copy.wait()
                    up_copy.wait()
            value = jnp.dot(h_v[block_rows(b), :], both_v[layer * chunks + c], preferred_element_type=F32)
            for e in range(2):
                at = e * half + brow
                acc[s, e * half : at + g, :] = value[e * half : at + g]
                for j in range(1, ny):
                    y1_snd[s, j - 1, e * g : (e + 1) * g, :] = value[at + j * g : at + (j + 1) * g].astype(BF16)
            for j in range(1, ny):
                y1_copy(s, j).start()

        valid1, s1, _, _, _ = item(t - LY)

        @pl.when(valid1)
        def _():
            for j in range(1, ny):
                y1_copy(s1, j).wait_recv()
            for e in range(2):
                mine = pl.ds(e * half + brow, g)
                total = acc[s1, mine, :]
                for j in range(1, ny):
                    total = total + y1_rcv[s1, j - 1, e * g : (e + 1) * g, :].astype(F32)
                acc[s1, mine, :] = total

        def chain(e, lag, snd, rcv, copy, base, size):
            at = place(e)
            ok, s, _, _, _ = item(t - lag - at * LZ)
            mine = pl.ds(e * half + base, size)

            @pl.when(ok & (at == 0))
            def _():
                snd[s, e] = acc[s, mine, :].astype(BF16)
                copy(s, e).start()

            @pl.when(ok & (at > 0) & (at < nz - 1))
            def _():
                copy(s, e).wait_recv()
                snd[s, e] = (acc[s, mine, :] + rcv[s, e].astype(F32)).astype(BF16)
                copy(s, e).start()

            @pl.when(ok & (at == nz - 1))
            def _():
                copy(s, e).wait_recv()
                acc[s, mine, :] += rcv[s, e].astype(F32)

        for e in range(2):
            chain(e, 0, cb_snd, cb_rcv, cb_copy, 0, brow)

        ok2, s2, _, _, _ = item(t - (nz - 1) * LZ)

        @pl.when(ok2 & is_end)
        def _():
            for j in range(1, ny):
                there = rows(end_base + lax.rem(y + j, ny) * g, g)
                y2_snd[s2, j - 1] = acc[s2, there, :].astype(BF16)
                y2_copy(s2, j).start()

        for e in range(2):
            chain(e, LY, ca_snd, ca_rcv, ca_copy, brow, g)

        ok3, s3, layer3, b3, c3 = item(t - p.act)

        @pl.when(ok3 & (c3 == 0) & (layer3 == 1))
        def _():
            scale[block_rows(b3), :] = factor_of(ms_snd, ms_rcv, ms_copy, 1, b3)

        @pl.when(ok3 & is_end)
        def _():
            def activate(value, row, to):
                factor = scale[rows(b3 * tb + row, g), 0:1]
                gv, uv = value[:, :cw] * factor, value[:, cw:] * factor
                hid[s3, rows(to, g), :] = (gv / (1.0 + jnp.exp(-gv)) * uv).astype(BF16)

            for j in range(1, ny):
                y2_copy(s3, j).wait_recv()
            own = end_base + y * g
            total = acc[s3, rows(own, g), :]
            for j in range(1, ny):
                total = total + y2_rcv[s3, j - 1].astype(F32)
            activate(total, own, own)
            for j in range(1, ny):
                h2_copy(s3, end_base, j, y).start()
            activate(acc[s3, rows(end_base + brow, g), :], end_base + brow + y * g, end_base + brow)
            for e in range(2):
                @pl.when(z == (nz - 1 if e else 0))
                def _():
                    ga_copy(s3, e).start()
                    for j in range(1, ny):
                        h1_copy(s3, e, j).start()

        for e in range(2):
            far = nz - 1 - place(e)
            ok, s, _, _, _ = item(t - p.act - far * LZ)

            @pl.when(ok & (far > 0))
            def _():
                ga_copy(s, e).wait_recv()
                for j in range(1, ny):
                    h1_copy(s, e, j).start()

            @pl.when(ok & (far > 0) & (far < nz - 1))
            def _():
                ga_copy(s, e).start()

        for e in range(2):
            far = nz - 1 - place(e)
            ok, s, _, _, _ = item(t - p.act - LY - far * LZ)

            @pl.when(ok & (far == 0))
            def _():
                for j in range(1, ny):
                    h2_copy(s, end_base, j, lax.rem(y + j, ny)).wait_recv()

            @pl.when(ok & (far > 0))
            def _():
                gb_copy(s, e).wait_recv()

            @pl.when(ok & (far < nz - 1))
            def _():
                gb_copy(s, e).start()

        ok4, s4, layer4, b4, c4 = item(t - p.down)

        @pl.when(ok4)
        def _():
            for e in range(2):
                for j in range(1, ny):
                    h1_copy(s4, e, j).wait_recv()
            for one in range(2):
                @pl.when((b4 == 0) & (layer4 == one))
                def _():
                    weights(one, c4)[2].wait()
            value = jnp.dot(hid[s4], down_v[layer4 * chunks + c4], preferred_element_type=F32)

            @pl.when(c4 == 0)
            def _():
                branch[block_rows(b4), :] = value

            @pl.when(c4 > 0)
            def _():
                branch[block_rows(b4), :] += value

            for j in range(1, ny):
                y1_copy(s4, j).wait_send()
                for e in range(2):
                    h1_copy(s4, e, j).wait_send()
            for e in range(2):
                @pl.when(place(e) < nz - 1)
                def _():
                    ca_copy(s4, e).wait_send()
                    cb_copy(s4, e).wait_send()

                @pl.when(place(e) > 0)
                def _():
                    ga_copy(s4, e).wait_send()
                    gb_copy(s4, e).wait_send()

            @pl.when(is_end)
            def _():
                for j in range(1, ny):
                    y2_copy(s4, j).wait_send()
                    h2_copy(s4, end_base, j, y).wait_send()

        def after(k):
            ok, _, layer, b, c = item(t - p.post[k])
            return ok & (c == chunks - 1), layer, b

        peer = col + 1 - 2 * core

        def d_copy(layer, b):
            away = branch.at[rows(b * tb + (1 - core) * half, half), :]
            return remote(away, d_rcv.at[layer, b], d_s.at[layer, b], d_r.at[layer, b], cb=peer)

        def x_copy(layer, b, k):
            bit = lax.rem(lax.div(col, 2 << k), 2)
            to = col + (1 - 2 * bit) * (2 << k)
            return remote(x_snd.at[layer, b, k], x_rcv.at[layer, b, k], x_s.at[layer, b, k], x_r.at[layer, b, k], cb=to)

        def t_copy(layer, b):
            part = tot.at[layer, b, rows(core * half, half), :]
            return remote(part, part, t_s.at[layer, b], t_r.at[layer, b], cb=peer)

        def whole(layer, b, total):
            base = core * half
            tot[layer, b, rows(base, brow), :] = total[:brow]
            for j in range(ny):
                to = base + brow + lax.rem(y + j, ny) * g
                tot[layer, b, rows(to, g), :] = total[brow + j * g : brow + (j + 1) * g]
            t_copy(layer, b).start()

        go, layer, b = after(0)

        @pl.when(go)
        def _():
            d_copy(layer, b).start()

        for k in range(p.kx + 1):
            go_k, layer_k, b_k = after(k + 1)

            @pl.when(go_k)
            def _():
                if k == 0:
                    d_copy(layer_k, b_k).wait()
                    total = branch[rows(b_k * tb + core * half, half), :] + d_rcv[layer_k, b_k]
                else:
                    x_copy(layer_k, b_k, k - 1).wait()
                    total = x_snd[layer_k, b_k, k - 1] + x_rcv[layer_k, b_k, k - 1]
                if k < p.kx:
                    x_snd[layer_k, b_k, k] = total
                    x_copy(layer_k, b_k, k).start()
                else:
                    whole(layer_k, b_k, total)

        go5, layer5, b5 = after(p.kx + 2)

        @pl.when(go5)
        def _():
            t_copy(layer5, b5).wait()
            br_snd[layer5, b5] = squares(tot[layer5, b5])
            for off in range(1, n):
                br_copy(layer5, b5, off).start()

        go6, layer6, b6 = after(p.kx + 3)

        for one in range(2):
            @pl.when(go6 & (layer6 == one))
            def _():
                factor = 0.5 * factor_of(br_snd, br_rcv, br_copy, one, b6)[:, 0:1]
                gain = (post1, post2)[one][...]
                middle = mid[block_rows(b6), :] + factor * tot[one, b6] * gain
                if one == 0:
                    mid[block_rows(b6), :] = middle
                    store_h(b6, middle * pre2[...])
                    ms_snd[1, b6] = squares(middle)
                    for off in range(1, n):
                        ms_copy(1, b6, off).start()
                else:
                    y_out[block_rows(b6), :] = middle.astype(BF16)

        return carry

    lax.fori_loop(0, p.ticks, tick, 0)


def solution(mesh):
    n, nc = mesh.shape["ra"], mesh.shape["cb"]

    def body(tokens, pre1, gate1, up1, down1, post1, pre2, gate2, up2, down2, post2):
        count, depth = tokens.shape
        p = Plan(n, nc, count, depth, gate1.shape[1])
        vmem = pl.BlockSpec(memory_space=pltpu.VMEM)
        hbm = pl.BlockSpec(memory_space=pl.ANY)
        dma = pltpu.SemaphoreType.DMA
        items, blocks, wide, ny = p.items, p.blocks, 2 * p.cw, p.ny
        scratch = [
            pltpu.VMEM((2 * p.chunks, depth, wide), BF16),
            pltpu.VMEM((2 * p.chunks, p.cw, depth), BF16),
            pltpu.VMEM((count, depth), BF16),
            pltpu.VMEM((count, depth), F32),
            pltpu.VMEM((items, p.tb, wide), F32),
            pltpu.VMEM((count, depth), F32),
            pltpu.VMEM((count, 128), F32),
            pltpu.VMEM((items, p.tb, p.cw), BF16),
        ]
        scratch += [pltpu.VMEM((items, ny - 1, 2 * p.g, wide), BF16)] * 2
        scratch += [pltpu.VMEM((items, 2, p.g, wide), BF16)] * 2
        scratch += [pltpu.VMEM((items, 2, ny * p.g, wide), BF16)] * 2
        scratch += [pltpu.VMEM((items, ny - 1, p.g, wide), BF16)] * 2
        scratch += [pltpu.VMEM((2, blocks, p.half, depth), F32)]
        scratch += [pltpu.VMEM((2, blocks, max(1, p.kx), p.half, depth), F32)] * 2
        scratch += [pltpu.VMEM((2, blocks, p.tb, depth), F32)]
        scratch += [pltpu.VMEM((2, blocks, 8, p.tb), F32), pltpu.VMEM((2, blocks, n - 1, 8, p.tb), F32)] * 2
        scratch += [dma((3, 2 * p.chunks))]
        scratch += [dma((ny - 1, items))] * 2 + [dma((2, items))] * 4 + [dma((ny - 1, items))] * 4
        scratch += [dma((2, items))] * 4 + [dma((2, ny - 1, items))] * 2
        scratch += [dma((2, blocks))] * 2 + [dma((2, blocks, max(1, p.kx)))] * 2 + [dma((2, blocks))] * 2
        scratch += [dma((2, blocks, n - 1))] * 4
        row = lambda gain: gain.reshape(1, depth)
        return pl.pallas_call(
            functools.partial(kernel, p, depth * n),
            out_shape=jax.ShapeDtypeStruct((count, depth), BF16),
            in_specs=[vmem] * 5 + [hbm] * 6,
            out_specs=vmem,
            scratch_shapes=scratch,
            compiler_params=pltpu.CompilerParams(
                collective_id=0, has_side_effects=True, vmem_limit_bytes=62 * 1024 * 1024
            ),
            name="both",
        )(tokens, row(pre1), row(post1), row(pre2), row(post2), gate1, up1, down1, gate2, up2, down2)

    in_specs = (
        P(None, "ra"), P("ra"), P("ra", "cb"), P("ra", "cb"), P("cb", "ra"), P("ra"),
        P("ra"), P("ra", "cb"), P("ra", "cb"), P("cb", "ra"), P("ra"),
    )
    return jax.shard_map(body, mesh=mesh, in_specs=in_specs, out_specs=P(None, "ra"), check_vma=False)
```

time: 241 us -> 200 us (0.83)
  Pallas kernels: 236 us -> 198 us
    pallas_call x2 -> x1, Pallas kernels: 236 us -> 198 us  [body(): pl.pallas_call(functools.partial(kernel, p, depth * n), out_shape=jax.Sha...]
where the time goes in v1:
time: 200 us
  Pallas kernels  198 us (99%)
    pallas_call x1, Pallas kernels, body(): pl.pallas_call(functools.partial(kernel, p, depth * n), out_shape=jax.Sha...  198 us

profile of v1, /device:TPU:0, one launch (start us, length us, event | category | flops | bytes accessed | tf_op | source)
XLA Modules:
  0.0 200.2 jit_solution(3606082647489021714)
XLA Ops:
  0.0 198.3 %both.1 = bf16[512,512]{1,0:T(8,128)(2,1)} custom-call(bf16[512,512]{1,0:T(8,128)(2,1)} %refs_0_.1, f32[1,512]{1,0:T(1,128)} %bitcast.4, f32[1,512]{1,0:T(1,128)} %bitcast.5, f32[1,512]{1,0:T(1,128)} %bitcast.6, f32[1,512]{1,0:T(1,128)} %bitcast.7, bf16[512,2816]{1,0:T(8,128)(2,1)} %refs_5_.1, bf16[512,2816]{1,0:T(8,128)(2,1)} %refs_6_.1, ...), custom_call_target="tpu_custom_call" | custom-call | tf_op jit(solution)/shard_map/both/pallas_call | solution.py:503
  198.3 1.9 copy.13

commit v2 on v1

--- a/solution.py
+++ b/solution.py
@@ -11,8 +11,8 @@
 MESH = pl.DeviceIdType.MESH
 F32 = jnp.float32
 BF16 = jnp.bfloat16
-LY, LZ = 3, 3
-POST = (2, 3, 2, 3)
+LY, LZ, MY, MZ = 3, 3, 3, 3
+POST = (2, 4, 2, 4)
 
 
 def log2(n):
@@ -20,11 +20,11 @@
 
 
 def spread(col):
-    return jnp.broadcast_to(col, (col.shape[0], 128)).T[0:8]
+    return jnp.broadcast_to(col, (col.shape[0], 128)).T[0:1]
 
 
 def column(row):
-    return jnp.broadcast_to(row[0:1], (128, row.shape[1])).T
+    return jnp.broadcast_to(row, (128, row.shape[1])).T
 
 
 class Plan:
@@ -39,7 +39,7 @@
         self.chunks, self.blocks = hidden // self.cw, tokens // self.tb
         self.items = self.chunks * self.blocks
         self.act = (self.nz - 1) * LZ + LY
-        self.down = self.act + LY + (self.nz - 1) * LZ
+        self.down = self.act + MY + (self.nz - 1) * MZ
         steps = [0, POST[0]] + [POST[1]] * self.kx + [POST[2], POST[3]]
         self.post = [self.down + sum(steps[: i + 1]) for i in range(len(steps))]
         self.gap = max(0, self.chunks + self.post[-1] - self.items)
@@ -81,11 +81,13 @@
             pltpu.make_async_copy(down.at[cols, :], down_v.at[k], w_sem.at[2, k]),
         ]
 
-    for layer in range(2):
+    def fetch(layer):
         @pl.loop(0, chunks)
         def _(c):
             for copy in weights(layer, c):
                 copy.start()
+
+    fetch(0)
 
     barrier = pltpu.get_barrier_semaphore()
     for off in range(1, n):
@@ -213,6 +215,7 @@
         @pl.when(t == chunks // 2)
         def _():
             prepare()
+            fetch(1)
 
         valid, s, layer, b, c = item(t)
 
@@ -314,7 +317,7 @@
 
         for e in range(2):
             far = nz - 1 - place(e)
-            ok, s, _, _, _ = item(t - p.act - far * LZ)
+            ok, s, _, _, _ = item(t - p.act - far * MZ)
 
             @pl.when(ok & (far > 0))
             def _():
@@ -328,7 +331,7 @@
 
         for e in range(2):
             far = nz - 1 - place(e)
-            ok, s, _, _, _ = item(t - p.act - LY - far * LZ)
+            ok, s, _, _, _ = item(t - p.act - MY - far * MZ)
 
             @pl.when(ok & (far == 0))
             def _():
@@ -493,7 +496,7 @@
         scratch += [pltpu.VMEM((2, blocks, p.half, depth), F32)]
         scratch += [pltpu.VMEM((2, blocks, max(1, p.kx), p.half, depth), F32)] * 2
         scratch += [pltpu.VMEM((2, blocks, p.tb, depth), F32)]
-        scratch += [pltpu.VMEM((2, blocks, 8, p.tb), F32), pltpu.VMEM((2, blocks, n - 1, 8, p.tb), F32)] * 2
+        scratch += [pltpu.VMEM((2, blocks, 1, p.tb), F32), pltpu.VMEM((2, blocks, n - 1, 1, p.tb), F32)] * 2
         scratch += [dma((3, 2 * p.chunks))]
         scratch += [dma((ny - 1, items))] * 2 + [dma((2, items))] * 4 + [dma((ny - 1, items))] * 4
         scratch += [dma((2, items))] * 4 + [dma((2, ny - 1, items))] * 2

time: 200 us -> 192 us (0.960)
  Pallas kernels: 198 us -> 190 us
    pallas_call x1, Pallas kernels: 198 us -> 190 us  [body(): pl.pallas_call(functools.partial(kernel, p, depth * n), out_shape=jax.Sha...]
where the time goes in v2:
time: 192 us
  Pallas kernels  190 us (99%)
    pallas_call x1, Pallas kernels, body(): pl.pallas_call(functools.partial(kernel, p, depth * n), out_shape=jax.Sha...  190 us

profile of v2, /device:TPU:0, one launch (start us, length us, event | category | flops | bytes accessed | tf_op | source)
XLA Modules:
  0.0 191.7 jit_solution(8285139063100918420)
XLA Ops:
  0.0 189.8 %both.1 = bf16[512,512]{1,0:T(8,128)(2,1)} custom-call(bf16[512,512]{1,0:T(8,128)(2,1)} %refs_0_.1, f32[1,512]{1,0:T(1,128)} %bitcast.4, f32[1,512]{1,0:T(1,128)} %bitcast.5, f32[1,512]{1,0:T(1,128)} %bitcast.6, f32[1,512]{1,0:T(1,128)} %bitcast.7, bf16[512,2816]{1,0:T(8,128)(2,1)} %refs_5_.1, bf16[512,2816]{1,0:T(8,128)(2,1)} %refs_6_.1, ...), custom_call_target="tpu_custom_call" | custom-call | tf_op jit(solution)/shard_map/both/pallas_call | solution.py:506
  189.8 1.9 copy.13

commit v3 on v2

v3 whole, which is shorter than its diff:
```python
import functools

import jax
import jax.numpy as jnp
from jax import lax
from jax.experimental import pallas as pl
from jax.experimental.pallas import tpu as pltpu
from jax.sharding import PartitionSpec as P

EPS = 1e-06
MESH = pl.DeviceIdType.MESH
F32 = jnp.float32
BF16 = jnp.bfloat16
LY, LZ, MY, MZ = 3, 3, 3, 3
POST = (2, 3, 4)


def log2(n):
    return n.bit_length() - 1


def spread(col):
    return jnp.broadcast_to(col, (col.shape[0], 128)).T[0:1]


def column(row):
    return jnp.broadcast_to(row, (128, row.shape[1])).T


class Plan:
    def __init__(self, n, nc, tokens, depth, hidden):
        self.n, self.nc, self.tokens, self.depth = n, nc, tokens, depth
        self.ny = 1 << (log2(n) // 2)
        self.nz = n // self.ny
        self.kx = log2(nc) - 1
        self.tb = 64 * self.ny
        self.half, self.g = self.tb // 2, 16
        self.lanes = max(self.half, 128)
        self.cw = 256 if hidden % 256 == 0 else 128
        self.chunks, self.blocks = hidden // self.cw, tokens // self.tb
        self.items = self.chunks * self.blocks
        self.act = (self.nz - 1) * LZ + LY
        self.down = self.act + MY + (self.nz - 1) * MZ
        steps = [0, POST[0]] + [POST[1]] * self.kx + [POST[2]]
        self.post = [self.down + sum(steps[: i + 1]) for i in range(len(steps))]
        self.gap = max(0, self.chunks + self.post[-1] - self.items)
        self.ticks = 2 * self.items + self.gap + self.post[-1]
        self.ring = self.items + self.gap + max(LY, MY)


def kernel(p, width, *refs):
    (tok_hbm, pre1, post1, pre2, post2, gate1, up1, down1, gate2, up2, down2, y_hbm), refs = refs[:12], refs[12:]
    (both_v, down_v, h_v, mid, acc, branch, scale, hid), refs = refs[:8], refs[8:]
    (yr_snd, yr_rcv, zr_snd, zr_rcv, ya_snd, ya_rcv, za), refs = refs[:7], refs[7:]
    (d_rcv, x_snd, x_rcv, tot, br_snd, br_rcv, ms_snd, ms_rcv), refs = refs[:8], refs[8:]
    (w_sem, yr_s, yr_r, zr_s, zr_r, ya_s, ya_r, za_s, za_r), refs = refs[:9], refs[9:]
    d_s, d_r, x_s, x_r, t_s, t_r, br_s, br_r, ms_s, ms_r, fac, tok, y_out, io_s = refs

    n, nc, ny, nz, tb, half, g, cw = p.n, p.nc, p.ny, p.nz, p.tb, p.half, p.g, p.cw
    chunks, blocks, items = p.chunks, p.blocks, p.items
    me, col = lax.axis_index("ra"), lax.axis_index("cb")
    z, y = lax.div(me, ny), lax.rem(me, ny)
    core = lax.rem(col, 2)
    brow = ny * g

    def remote(src, dst, s, r, **where):
        return pltpu.make_async_remote_copy(
            src_ref=src, dst_ref=dst, send_sem=s, recv_sem=r, device_id=where, device_id_type=MESH
        )

    def rows(base, size):
        return pl.ds(pl.multiple_of(base, 16), size)

    def weights(layer, c):
        cols = pl.ds(pl.multiple_of(c * cw, 128), cw)
        gate, up, down = ((gate1, up1, down1), (gate2, up2, down2))[layer]
        k = layer * chunks + c
        return [
            pltpu.make_async_copy(gate.at[:, cols], both_v.at[k, :, pl.ds(0, cw)], w_sem.at[0, k]),
            pltpu.make_async_copy(up.at[:, cols], both_v.at[k, :, pl.ds(cw, cw)], w_sem.at[1, k]),
            pltpu.make_async_copy(down.at[cols, :], down_v.at[k], w_sem.at[2, k]),
        ]

    def fetch(layer, start):
        @pl.loop(start, chunks)
        def _(c):
            for copy in weights(layer, c):
                copy.start()

    tok_copy = pltpu.make_async_copy(tok_hbm, tok, io_s.at[0])
    tok_copy.start()
    for copy in weights(0, 0):
        copy.start()
    barrier = pltpu.get_barrier_semaphore()
    for off in range(1, n):
        pl.semaphore_signal(barrier, inc=1, device_id={"ra": lax.rem(me + off, n)}, device_id_type=MESH)
    for off in range(1, nc):
        pl.semaphore_signal(barrier, inc=1, device_id={"cb": lax.rem(col + off, nc)}, device_id_type=MESH)

    fetch(0, 1)

    def other_y(j):
        return z * ny + lax.rem(y + j, ny)

    def next_z(e):
        return lax.rem(z + (1 if e else nz - 1), nz) * ny + y

    def back_z(e):
        return lax.rem(z + (nz - 1 if e else 1), nz) * ny + y

    def place(e):
        return z if e else nz - 1 - z

    def yr_copy(slot, j, part):
        return remote(
            yr_snd.at[slot, j - 1, pl.ds(*part), :], yr_rcv.at[slot, ny - 1 - j, pl.ds(*part), :],
            yr_s.at[j - 1, slot], yr_r.at[ny - 1 - j, slot], ra=other_y(j),
        )

    def ya_copy(slot, j, part):
        return remote(
            ya_snd.at[slot, pl.ds(*part), :], ya_rcv.at[slot, ny - 1 - j, pl.ds(*part), :],
            ya_s.at[j - 1, slot], ya_r.at[ny - 1 - j, slot], ra=other_y(j),
        )

    def zr_copy(slot, e):
        return remote(zr_snd.at[slot, e], zr_rcv.at[slot, e], zr_s.at[e, slot], zr_r.at[e, slot], ra=next_z(e))

    def za_copy(slot, e):
        return remote(za.at[slot, e], za.at[slot, e], za_s.at[e, slot], za_r.at[e, slot], ra=back_z(e))

    def by_part(one, two, act):
        for ok, part in ((one & two, (0, 3 * g)), (one & ~two, (0, 2 * g)), (two & ~one, (2 * g, g))):
            @pl.when(ok)
            def _():
                for j in range(1, ny):
                    act(j, part)

    def ms_copy(layer, b, off):
        return remote(
            ms_snd.at[layer, b], ms_rcv.at[layer, b, n - 1 - off],
            ms_s.at[layer, b, off - 1], ms_r.at[layer, b, n - 1 - off], ra=lax.rem(me + off, n),
        )

    def br_copy(layer, b, off, across):
        start = n - 1 if across else -1
        to = start + (n - off) % n
        where = {"cb": col + 1 - 2 * core} if across else {}
        return remote(
            br_snd.at[layer, b], br_rcv.at[layer, b, to],
            br_s.at[layer, b, start + off], br_r.at[layer, b, to], ra=lax.rem(me + off, n), **where,
        )

    br_all = [(off, False) for off in range(1, n)] + [(off, True) for off in range(n)]

    def store_h(b, value):
        value = value.astype(BF16)
        for e in range(2):
            h_v[rows(b * tb + e * half, brow), :] = value[e * half : e * half + brow]
            for yy in range(ny):
                slot = lax.rem(yy - y + ny, ny)
                at = e * half + brow + yy * g
                h_v[rows(b * tb + e * half + brow + slot * g, g), :] = value[at : at + g]

    def squares(value):
        return spread(jnp.sum(value * value, axis=1, keepdims=True))

    def block_rows(b):
        return pl.ds(pl.multiple_of(b * tb, tb), tb)

    def start_blocks(b):
        value = tok[block_rows(b), :].astype(F32)
        mid[block_rows(b), :] = value
        ms_snd[0, b] = squares(value)

    tok_copy.wait()
    for b in range(blocks):
        start_blocks(b)
    store_h(0, mid[0:tb, :] * pre1[...])

    pl.semaphore_wait(barrier, n - 1 + nc - 1)

    def factor_of(layer, b):
        for off in range(1, n):
            ms_copy(layer, b, off).wait()
        total = ms_snd[layer, b]
        for off in range(1, n):
            total = total + ms_rcv[layer, b, off - 1]
        return column(lax.rsqrt(total / width + EPS))

    def prepare():
        for b in range(blocks):
            factor = factor_of(0, b)
            if b == 0:
                scale[block_rows(b), :] = factor
            else:
                scale[block_rows(b), :] = jnp.ones_like(factor)
                store_h(b, mid[block_rows(b), :] * factor[:, 0:1] * pre1[...])

    is_end = (z == 0) | (z == nz - 1)
    end = jnp.where(z == 0, 0, 1)
    last = nz - 1

    def item(u):
        later = u >= items + p.gap
        valid = ((u >= 0) & (u < items)) | (later & (u < 2 * items + p.gap))
        s = u - jnp.where(later, items + p.gap, 0)
        layer = jnp.where(later, 1, 0)
        b = lax.div(s, chunks)
        return valid, s, layer, b, s - b * chunks

    def y_copy(b):
        return pltpu.make_async_copy(y_out.at[block_rows(b), :], y_hbm.at[block_rows(b), :], io_s.at[1 + b])

    def slot_of(v):
        return lax.rem(jnp.maximum(v, 0), p.ring)

    def valid(u):
        return item(u)[0]

    def tick(t, carry):
        x = t - p.act
        y_slot, y_old = slot_of(t), slot_of(t - LY)
        g_slot, g_old = slot_of(x), slot_of(x - MY)

        @pl.when(t == chunks // 2)
        def _():
            prepare()
            fetch(1, 0)

        ok, s, layer, b, c = item(t)

        @pl.when(ok)
        def _():
            for one in range(2):
                @pl.when((b == 0) & (layer == one))
                def _():
                    gate_copy, up_copy, _ = weights(one, c)
                    gate_copy.wait()
                    up_copy.wait()
            value = jnp.dot(h_v[block_rows(b), :], both_v[layer * chunks + c], preferred_element_type=F32)
            for e in range(2):
                at = e * half + brow
                acc[s, e * half : at + g, :] = value[e * half : at + g]
                for j in range(1, ny):
                    yr_snd[y_slot, j - 1, e * g : (e + 1) * g, :] = value[at + j * g : at + (j + 1) * g].astype(BF16)

        by_part(
            valid(t - LY), is_end & valid(t - LY - last * LZ), lambda j, part: yr_copy(y_old, j, part).wait()
        )
        ok1, s1, _, _, _ = item(t - LY)

        @pl.when(ok1)
        def _():
            for e in range(2):
                mine = pl.ds(e * half + brow, g)
                total = acc[s1, mine, :]
                for j in range(1, ny):
                    total = total + yr_rcv[y_old, j - 1, e * g : (e + 1) * g, :].astype(F32)
                acc[s1, mine, :] = total

        for e in range(2):
            at = place(e)
            v = t - at * LZ
            now, old = slot_of(v), slot_of(v - LZ)
            ok_b, s_b, _, _, _ = item(v)
            ok_a, s_a, _, _, _ = item(v - LY)

            @pl.when((ok_b | ok_a) & (at > 0))
            def _():
                zr_copy(now, e).wait_recv()

            for ok_i, s_i, base, size in ((ok_b, s_b, 0, brow), (ok_a, s_a, brow, g)):
                mine, part = pl.ds(e * half + base, size), pl.ds(base, size)

                @pl.when(ok_i & (at == 0))
                def _():
                    zr_snd[now, e, part, :] = acc[s_i, mine, :].astype(BF16)

                @pl.when(ok_i & (at > 0) & (at < last))
                def _():
                    zr_snd[now, e, part, :] = (
                        acc[s_i, mine, :] + zr_rcv[now, e, part, :].astype(F32)
                    ).astype(BF16)

                @pl.when(ok_i & (at == last))
                def _():
                    acc[s_i, mine, :] += zr_rcv[now, e, part, :].astype(F32)

            @pl.when((ok_b | ok_a) & (at < last))
            def _():
                zr_copy(now, e).start()

            @pl.when((valid(v - LZ) | valid(v - LZ - LY)) & (at < last))
            def _():
                zr_copy(old, e).wait_send()

        ok2, s2, _, _, _ = item(t - last * LZ)

        @pl.when(ok2 & is_end)
        def _():
            for j in range(1, ny):
                there = rows(end * half + lax.rem(y + j, ny) * g, g)
                yr_snd[y_slot, j - 1, 2 * g :, :] = acc[s2, there, :].astype(BF16)

        by_part(ok, ok2 & is_end, lambda j, part: yr_copy(y_slot, j, part).start())

        ok3, s3, layer3, b3, c3 = item(x)

        @pl.when(ok3 & (c3 == 0) & (layer3 == 1))
        def _():
            scale[block_rows(b3), :] = factor_of(1, b3)

        @pl.when(ok3 & is_end)
        def _():
            def activate(value, row):
                factor = scale[rows(b3 * tb + row, g), 0:1]
                gv, uv = value[:, :cw] * factor, value[:, cw:] * factor
                return (gv / (1.0 + jnp.exp(-gv)) * uv).astype(BF16)

            own = end * half + y * g
            total = acc[s3, rows(own, g), :]
            for j in range(1, ny):
                total = total + yr_rcv[y_old, j - 1, 2 * g :, :].astype(F32)
            value = activate(total, own)
            hid[s3, rows(own, g), :] = value
            ya_snd[g_slot, 2 * g :, :] = value
            own = rows(end * half + brow, g)
            hid[s3, own, :] = activate(acc[s3, own, :], end * half + brow + y * g)

        by_part(
            valid(x - MY - last * MZ), is_end & valid(x - MY), lambda j, part: ya_copy(g_old, j, part).wait()
        )
        ok4, s4, layer4, b4, c4 = item(t - p.down)
        ok5, s5, _, _, _ = item(x - MY)

        @pl.when(ok4)
        def _():
            for e in range(2):
                for j in range(1, ny):
                    to = e * half + brow + j * g
                    hid[s4, to : to + g, :] = ya_rcv[g_old, j - 1, e * g : (e + 1) * g, :]

        @pl.when(ok5 & is_end)
        def _():
            for j in range(1, ny):
                hid[s5, rows(end * half + lax.rem(y + j, ny) * g, g), :] = ya_rcv[g_old, j - 1, 2 * g :, :]

        for e in range(2):
            far = last - place(e)
            w = x - far * MZ
            now, old = slot_of(w), slot_of(w - MZ)
            ok_a, s_a, _, _, _ = item(w)
            ok_b, s_b, _, _, _ = item(w - MY)

            @pl.when((ok_a | ok_b) & (far > 0))
            def _():
                za_copy(now, e).wait_recv()

            for ok_i, s_i, base, size in ((ok_b, s_b, 0, brow), (ok_a, s_a, brow, g)):
                mine, part = pl.ds(e * half + base, size), pl.ds(base, size)

                @pl.when(ok_i & (far == 0))
                def _():
                    za[now, e, part, :] = hid[s_i, mine, :]

            @pl.when((ok_a | ok_b) & (far < last))
            def _():
                za_copy(now, e).start()

            for ok_i, s_i, base, size in ((ok_b, s_b, 0, brow), (ok_a, s_a, brow, g)):
                mine, part = pl.ds(e * half + base, size), pl.ds(base, size)

                @pl.when(ok_i & (far > 0))
                def _():
                    hid[s_i, mine, :] = za[now, e, part, :]

            @pl.when((valid(w - MZ) | valid(w - MZ - MY)) & (far < last))
            def _():
                za_copy(old, e).wait_send()

        ok6, s6, _, _, _ = item(x - last * MZ)

        @pl.when(ok6)
        def _():
            for e in range(2):
                at = e * half + brow
                ya_snd[g_slot, e * g : (e + 1) * g, :] = hid[s6, at : at + g, :]

        by_part(ok6, ok3 & is_end, lambda j, part: ya_copy(g_slot, j, part).start())

        @pl.when(ok4)
        def _():
            for one in range(2):
                @pl.when((b4 == 0) & (layer4 == one))
                def _():
                    weights(one, c4)[2].wait()
            value = jnp.dot(hid[s4], down_v[layer4 * chunks + c4], preferred_element_type=F32)

            @pl.when(c4 == 0)
            def _():
                branch[block_rows(b4), :] = value

            @pl.when(c4 > 0)
            def _():
                branch[block_rows(b4), :] += value

        @pl.when(t == 0)
        def _():
            for b in range(blocks):
                for off in range(1, n):
                    ms_copy(0, b, off).start()

        def after(k):
            ok, _, layer, b, c = item(t - p.post[k])
            return ok & (c == chunks - 1), layer, b

        peer = col + 1 - 2 * core

        def d_copy(layer, b):
            away = branch.at[rows(b * tb + (1 - core) * half, half), :]
            return remote(away, d_rcv.at[layer, b], d_s.at[layer, b], d_r.at[layer, b], cb=peer)

        def x_copy(layer, b, k):
            bit = lax.rem(lax.div(col, 2 << k), 2)
            to = col + (1 - 2 * bit) * (2 << k)
            return remote(x_snd.at[layer, b, k], x_rcv.at[layer, b, k], x_s.at[layer, b, k], x_r.at[layer, b, k], cb=to)

        def t_copy(layer, b):
            part = tot.at[layer, b, rows(core * half, half), :]
            return remote(part, part, t_s.at[layer, b], t_r.at[layer, b], cb=peer)

        def whole(layer, b, total):
            base = core * half
            tot[layer, b, rows(base, brow), :] = total[:brow]
            for j in range(ny):
                to = base + brow + lax.rem(y + j, ny) * g
                tot[layer, b, rows(to, g), :] = total[brow + j * g : brow + (j + 1) * g]
            t_copy(layer, b).start()
            value = tot[layer, b, rows(base, half), :]
            sums = jnp.sum(value * value, axis=1, keepdims=True)
            if p.lanes > half:
                sums = jnp.concatenate([sums, jnp.zeros((p.lanes - half, 1), F32)], axis=0)
            br_snd[layer, b] = spread(sums)
            for off, across in br_all:
                br_copy(layer, b, off, across).start()

        go, layer, b = after(0)

        @pl.when(go)
        def _():
            d_copy(layer, b).start()

        for k in range(p.kx + 1):
            go_k, layer_k, b_k = after(k + 1)

            @pl.when(go_k)
            def _():
                if k == 0:
                    d_copy(layer_k, b_k).wait()
                    total = branch[rows(b_k * tb + core * half, half), :] + d_rcv[layer_k, b_k]
                else:
                    x_copy(layer_k, b_k, k - 1).wait()
                    total = x_snd[layer_k, b_k, k - 1].astype(F32) + x_rcv[layer_k, b_k, k - 1].astype(F32)
                if k < p.kx:
                    x_snd[layer_k, b_k, k] = total.astype(BF16)
                    x_copy(layer_k, b_k, k).start()
                else:
                    whole(layer_k, b_k, total)

        go6, layer6, b6 = after(p.kx + 2)

        for one in range(2):
            @pl.when(go6 & (layer6 == one))
            def _():
                t_copy(one, b6).wait()
                for off, across in br_all:
                    br_copy(one, b6, off, across).wait()
                own, other = br_snd[one, b6], br_rcv[one, b6, n - 1]
                for off in range(1, n):
                    own = own + br_rcv[one, b6, off - 1]
                    other = other + br_rcv[one, b6, n - 1 + off]
                for base, total in ((core * half, own), ((1 - core) * half, other)):
                    fac[rows(base, half), :] = column(0.5 * lax.rsqrt(total / width + EPS))[:half]
                factor = fac[:, 0:1]
                gain = (post1, post2)[one][...]
                middle = mid[block_rows(b6), :] + factor * tot[one, b6] * gain
                if one == 0:
                    mid[block_rows(b6), :] = middle
                    store_h(b6, middle * pre2[...])
                    ms_snd[1, b6] = squares(middle)
                    for off in range(1, n):
                        ms_copy(1, b6, off).start()
                else:
                    y_out[block_rows(b6), :] = middle.astype(BF16)
                    y_copy(b6).start()

        return carry

    lax.fori_loop(0, p.ticks, tick, 0)
    for b in range(blocks):
        y_copy(b).wait()


def solution(mesh):
    n, nc = mesh.shape["ra"], mesh.shape["cb"]

    def body(tokens, pre1, gate1, up1, down1, post1, pre2, gate2, up2, down2, post2):
        count, depth = tokens.shape
        p = Plan(n, nc, count, depth, gate1.shape[1])
        vmem = pl.BlockSpec(memory_space=pltpu.VMEM)
        hbm = pl.BlockSpec(memory_space=pl.ANY)
        dma = pltpu.SemaphoreType.DMA
        items, blocks, wide, ny = p.items, p.blocks, 2 * p.cw, p.ny
        scratch = [
            pltpu.VMEM((2 * p.chunks, depth, wide), BF16),
            pltpu.VMEM((2 * p.chunks, p.cw, depth), BF16),
            pltpu.VMEM((count, depth), BF16),
            pltpu.VMEM((count, depth), F32),
            pltpu.VMEM((items, p.tb, wide), F32),
            pltpu.VMEM((count, depth), F32),
            pltpu.VMEM((count, 128), F32),
            pltpu.VMEM((items, p.tb, p.cw), BF16),
        ]
        ring, many = p.ring, (ny + 1) * p.g
        scratch += [pltpu.VMEM((ring, ny - 1, 3 * p.g, wide), BF16)] * 2
        scratch += [pltpu.VMEM((ring, 2, many, wide), BF16)] * 2
        scratch += [pltpu.VMEM((ring, 3 * p.g, p.cw), BF16), pltpu.VMEM((ring, ny - 1, 3 * p.g, p.cw), BF16)]
        scratch += [pltpu.VMEM((ring, 2, many, p.cw), BF16)]
        scratch += [pltpu.VMEM((2, blocks, p.half, depth), F32)]
        scratch += [pltpu.VMEM((2, blocks, max(1, p.kx), p.half, depth), BF16)] * 2
        scratch += [pltpu.VMEM((2, blocks, p.tb, depth), F32)]
        scratch += [pltpu.VMEM((2, blocks, 1, p.lanes), F32), pltpu.VMEM((2, blocks, 2 * n - 1, 1, p.lanes), F32)]
        scratch += [pltpu.VMEM((2, blocks, 1, p.tb), F32), pltpu.VMEM((2, blocks, n - 1, 1, p.tb), F32)]
        scratch += [dma((3, 2 * p.chunks))]
        scratch += ([dma((ny - 1, ring))] * 2 + [dma((2, ring))] * 2) * 2
        scratch += [dma((2, blocks))] * 2 + [dma((2, blocks, max(1, p.kx)))] * 2 + [dma((2, blocks))] * 2
        scratch += [dma((2, blocks, 2 * n - 1))] * 2 + [dma((2, blocks, n - 1))] * 2
        scratch += [pltpu.VMEM((p.tb, 128), F32)] + [pltpu.VMEM((count, depth), BF16)] * 2 + [dma((1 + blocks,))]
        row = lambda gain: gain.reshape(1, depth)
        return pl.pallas_call(
            functools.partial(kernel, p, depth * n),
            out_shape=jax.ShapeDtypeStruct((count, depth), BF16),
            in_specs=[hbm] + [vmem] * 4 + [hbm] * 6,
            out_specs=hbm,
            scratch_shapes=scratch,
            compiler_params=pltpu.CompilerParams(
                collective_id=0, has_side_effects=True, vmem_limit_bytes=62 * 1024 * 1024
            ),
            name="both",
        )(tokens, row(pre1), row(post1), row(pre2), row(post2), gate1, up1, down1, gate2, up2, down2)

    in_specs = (
        P(None, "ra"), P("ra"), P("ra", "cb"), P("ra", "cb"), P("cb", "ra"), P("ra"),
        P("ra"), P("ra", "cb"), P("ra", "cb"), P("cb", "ra"), P("ra"),
    )
    return jax.shard_map(body, mesh=mesh, in_specs=in_specs, out_specs=P(None, "ra"), check_vma=False)
```

time: 192 us -> 191 us (level)
  no operation moved by 1% of the time
where the time goes in v3:
time: 191 us
  Pallas kernels  189 us (99%)
    pallas_call x1, Pallas kernels, body(): pl.pallas_call(functools.partial(kernel, p, depth * n), out_shape=jax.Sha...  189 us

profile of v3, /device:TPU:0, one launch (start us, length us, event | category | flops | bytes accessed | tf_op | source)
XLA Modules:
  0.0 190.9 jit_solution(864255195784637272)
XLA Ops:
  0.0 189.0 %both.1 = bf16[512,512]{1,0:T(8,128)(2,1)} custom-call(bf16[512,512]{1,0:T(8,128)(2,1)} %refs_0_.1, f32[1,512]{1,0:T(1,128)} %bitcast.4, f32[1,512]{1,0:T(1,128)} %bitcast.5, f32[1,512]{1,0:T(1,128)} %bitcast.6, f32[1,512]{1,0:T(1,128)} %bitcast.7, bf16[512,2816]{1,0:T(8,128)(2,1)} %refs_5_.1, bf16[512,2816]{1,0:T(8,128)(2,1)} %refs_6_.1, ...), custom_call_target="tpu_custom_call" | custom-call | tf_op jit(solution)/shard_map/both/pallas_call | solution.py:541
  189.0 1.9 copy.13

commit v4 on v3

--- a/solution.py
+++ b/solution.py
@@ -12,7 +12,7 @@
 F32 = jnp.float32
 BF16 = jnp.bfloat16
 LY, LZ, MY, MZ = 3, 3, 3, 3
-POST = (2, 3, 4)
+POST = (1, 3, 5)
 
 
 def log2(n):
@@ -123,11 +123,19 @@
             ya_s.at[j - 1, slot], ya_r.at[ny - 1 - j, slot], ra=other_y(j),
         )
 
-    def zr_copy(slot, e):
-        return remote(zr_snd.at[slot, e], zr_rcv.at[slot, e], zr_s.at[e, slot], zr_r.at[e, slot], ra=next_z(e))
-
-    def za_copy(slot, e):
-        return remote(za.at[slot, e], za.at[slot, e], za_s.at[e, slot], za_r.at[e, slot], ra=back_z(e))
+    def zr_copy(slot, e, part):
+        there = (slot, e, pl.ds(*part), slice(None))
+        return remote(zr_snd.at[there], zr_rcv.at[there], zr_s.at[e, slot], zr_r.at[e, slot], ra=next_z(e))
+
+    def za_copy(slot, e, part):
+        there = za.at[slot, e, pl.ds(*part), :]
+        return remote(there, there, za_s.at[e, slot], za_r.at[e, slot], ra=back_z(e))
+
+    def by_type(both, here, act):
+        for ok, part in ((both[0] & both[1], (0, brow + g)), (both[0] & ~both[1], (0, brow)), (both[1] & ~both[0], (brow, g))):
+            @pl.when(ok & here)
+            def _():
+                act(part)
 
     def by_part(one, two, act):
         for ok, part in ((one & two, (0, 3 * g)), (one & ~two, (0, 2 * g)), (two & ~one, (2 * g, g))):
@@ -266,9 +274,7 @@
             ok_b, s_b, _, _, _ = item(v)
             ok_a, s_a, _, _, _ = item(v - LY)
 
-            @pl.when((ok_b | ok_a) & (at > 0))
-            def _():
-                zr_copy(now, e).wait_recv()
+            by_type((ok_b, ok_a), at > 0, lambda part: zr_copy(now, e, part).wait_recv())
 
             for ok_i, s_i, base, size in ((ok_b, s_b, 0, brow), (ok_a, s_a, brow, g)):
                 mine, part = pl.ds(e * half + base, size), pl.ds(base, size)
@@ -287,13 +293,10 @@
                 def _():
                     acc[s_i, mine, :] += zr_rcv[now, e, part, :].astype(F32)
 
-            @pl.when((ok_b | ok_a) & (at < last))
-            def _():
-                zr_copy(now, e).start()
-
-            @pl.when((valid(v - LZ) | valid(v - LZ - LY)) & (at < last))
-            def _():
-                zr_copy(old, e).wait_send()
+            by_type((ok_b, ok_a), at < last, lambda part: zr_copy(now, e, part).start())
+            by_type(
+                (valid(v - LZ), valid(v - LZ - LY)), at < last, lambda part: zr_copy(old, e, part).wait_send()
+            )
 
         ok2, s2, _, _, _ = item(t - last * LZ)
 
@@ -353,9 +356,7 @@
             ok_a, s_a, _, _, _ = item(w)
             ok_b, s_b, _, _, _ = item(w - MY)
 
-            @pl.when((ok_a | ok_b) & (far > 0))
-            def _():
-                za_copy(now, e).wait_recv()
+            by_type((ok_b, ok_a), far > 0, lambda part: za_copy(now, e, part).wait_recv())
 
             for ok_i, s_i, base, size in ((ok_b, s_b, 0, brow), (ok_a, s_a, brow, g)):
                 mine, part = pl.ds(e * half + base, size), pl.ds(base, size)
@@ -364,9 +365,7 @@
                 def _():
                     za[now, e, part, :] = hid[s_i, mine, :]
 
-            @pl.when((ok_a | ok_b) & (far < last))
-            def _():
-                za_copy(now, e).start()
+            by_type((ok_b, ok_a), far < last, lambda part: za_copy(now, e, part).start())
 
             for ok_i, s_i, base, size in ((ok_b, s_b, 0, brow), (ok_a, s_a, brow, g)):
                 mine, part = pl.ds(e * half + base, size), pl.ds(base, size)
@@ -375,9 +374,9 @@
                 def _():
                     hid[s_i, mine, :] = za[now, e, part, :]
 
-            @pl.when((valid(w - MZ) | valid(w - MZ - MY)) & (far < last))
-            def _():
-                za_copy(old, e).wait_send()
+            by_type(
+                (valid(w - MZ - MY), valid(w - MZ)), far < last, lambda part: za_copy(old, e, part).wait_send()
+            )
 
         ok6, s6, _, _, _ = item(x - last * MZ)
 

time: 191 us -> 188 us (0.984)
  Pallas kernels: 189 us -> 185 us
    pallas_call x1, Pallas kernels: 189 us -> 185 us  [body(): pl.pallas_call(functools.partial(kernel, p, depth * n), out_shape=jax.Sha...]
where the time goes in v4:
time: 188 us; the launch traced here: 187 us
  Pallas kernels  185 us (98%)
    pallas_call x1, Pallas kernels, body(): pl.pallas_call(functools.partial(kernel, p, depth * n), out_shape=jax.Sha...  185 us

profile of v4, /device:TPU:0, one launch (start us, length us, event | category | flops | bytes accessed | tf_op | source)
XLA Modules:
  0.0 187.3 jit_solution(12398545305025782878)
XLA Ops:
  0.0 185.5 %both.1 = bf16[512,512]{1,0:T(8,128)(2,1)} custom-call(bf16[512,512]{1,0:T(8,128)(2,1)} %refs_0_.1, f32[1,512]{1,0:T(1,128)} %bitcast.4, f32[1,512]{1,0:T(1,128)} %bitcast.5, f32[1,512]{1,0:T(1,128)} %bitcast.6, f32[1,512]{1,0:T(1,128)} %bitcast.7, bf16[512,2816]{1,0:T(8,128)(2,1)} %refs_5_.1, bf16[512,2816]{1,0:T(8,128)(2,1)} %refs_6_.1, ...), custom_call_target="tpu_custom_call" | custom-call | tf_op jit(solution)/shard_map/both/pallas_call | solution.py:540
  185.5 1.9 copy.13
